TPU v7x, 32 devices: a whole 2x2x4 slice. The times are simulated.
32 devices in a mesh: sp: 8 (over z, x), tp: 4 (over y, core).
Axes of the slice: x: 2, y: 2, z: 4, core: 2. Of those that a mesh axis runs over, the one named last changes fastest.
Arguments:
- stream_in: bfloat16 [2048, 2048], P(('sp', 'tp')), may hold values from -6 to 6
- pre_gate: bfloat16 [2048, 1024], P('sp', 'tp'), may hold values from -6 to 6
- value_in: bfloat16 [2048, 1024], P('sp', 'tp'), may hold values from -6 to 6
- post_gate: bfloat16 [2048, 1024], P('sp', 'tp'), may hold values from -6 to 6
- conv_taps: bfloat16 [3, 1024], P(None, 'tp'), may hold values from -3 to 3
- out_weight: bfloat16 [1024, 2048], P('tp'), may hold values from -0.1875 to 0.1875
- route_ids: int32 [2048, 4], P('sp'), may hold values from 0 to 7, all different within a row; in each aligned block of 64 rows (0 to 63, 64 to 127, ...) at most 64 rows name the same one
- route_weight: float32 [2048, 4], P('sp'), may hold values from 0.1 to 1
- ffn_gain: bfloat16 [2048], replicated, may hold values from 0.099609375 to 1.8984375
- post_gain: bfloat16 [2048], replicated, may hold values from 0.099609375 to 1.8984375
- gate_proj: bfloat16 [8, 2048, 2048], P('sp', None, 'tp'), may hold values from -0.39648438 to 0.39648438
- up_proj: bfloat16 [8, 2048, 2048], P('sp', None, 'tp'), may hold values from -0.39648438 to 0.39648438
- down_proj: bfloat16 [8, 2048, 2048], P('sp', None, 'tp'), may hold values from -0.125 to 0.125
Outputs:
- layer_out: bfloat16 [2048, 2048], P(('sp', 'tp'))
Inputs may be any that keep to these rules, and one draw needn't show every extreme that they name: `route_ids`: in each aligned block of 64 positions, a row names 4 different experts and no expert is named by more than 64 rows; in every draw some expert reaches 64 in some block.
All inputs are finite; a program needn't handle non-finite values.
Results may differ from a plain program's by a relative error of at most 0.014.
Values may be sent and summed in bfloat16 or wider, within the bound.
A program may use at most 64 MiB of HBM per device.

v0:
```python
import jax
import jax.numpy as jnp
from jax import lax
from jax.sharding import PartitionSpec as P

clamp_limit = 7.0
sigmoid_scale = 1.702
epsilon = 1e-06


def passed_along(array, axis, by):
    count = lax.axis_size(axis)
    pairs = [(i, i + by) for i in range(count) if 0 <= i + by < count]
    return lax.ppermute(array, axis, pairs)


def clamped_units(gate_pre, up_pre):
    gate_cut = jnp.minimum(gate_pre, clamp_limit)
    up_cut = jnp.clip(up_pre, -clamp_limit, clamp_limit)
    return (up_cut + 1.0) * (gate_cut * jax.nn.sigmoid(sigmoid_scale * gate_cut))


def scaled_norm(values, gain):
    return (
        values
        * lax.rsqrt(jnp.mean(values * values, axis=-1, keepdims=True) + epsilon)
        * gain.astype(jnp.float32)
    )


def block_ranks(route_rows, experts, block_rows):
    flattened = route_rows.reshape(-1)
    entries = flattened.shape[0]
    span_width = block_rows * route_rows.shape[1]
    onehot = (flattened[:, None] == jnp.arange(experts, dtype=jnp.int32)[None, :]).astype(jnp.int32)
    blocked = onehot.reshape(entries // span_width, span_width, experts)
    before = jnp.cumsum(blocked, axis=1) - blocked
    return jnp.sum(before * blocked, axis=2).reshape(route_rows.shape)


def slot_picker(slot_index, table_size):
    matches = slot_index[None, :, :] == jnp.arange(table_size, dtype=jnp.int32)[:, None, None]
    return jnp.any(matches, axis=2).astype(jnp.bfloat16)


def local(
    stream_in,
    pre_gate,
    value_in,
    post_gate,
    conv_taps,
    out_weight,
    route_ids,
    route_weight,
    ffn_gain,
    post_gain,
    gate_proj,
    up_proj,
    down_proj,
):
    sp_count = lax.axis_size("sp")
    tp_count = lax.axis_size("tp")
    seq_rows = pre_gate.shape[0]
    own_rows = seq_rows // tp_count
    top_count = route_ids.shape[1]
    slots_each = 2 * own_rows * top_count // sp_count
    tap_count = conv_taps.shape[0]
    gated_input = (pre_gate.astype(jnp.float32) * value_in.astype(jnp.float32)).astype(jnp.bfloat16)
    rim_rows = passed_along(gated_input[seq_rows - tap_count + 1 :], "sp", 1)
    padded = jnp.concatenate([rim_rows, gated_input], 0).astype(jnp.float32)
    convolved = jnp.zeros(gated_input.shape, jnp.float32)
    for tap_index in range(tap_count):
        convolved = (
            convolved
            + conv_taps[tap_index].astype(jnp.float32)[None, :]
            * padded[tap_index : tap_index + seq_rows]
        )
    mixer_out = (post_gate.astype(jnp.float32) * convolved).astype(jnp.bfloat16)
    weight_rows = mixer_out
    projected = lax.psum_scatter(
        jnp.dot(weight_rows, out_weight, preferred_element_type=jnp.float32),
        "tp",
        scatter_dimension=0,
        tiled=True,
    )
    residual = (stream_in.astype(jnp.float32) + projected).astype(jnp.bfloat16)
    normed = scaled_norm(residual.astype(jnp.float32), ffn_gain).astype(jnp.bfloat16)
    slot_rank = block_ranks(route_ids, sp_count, own_rows)
    block_of = (jnp.arange(seq_rows, dtype=jnp.int32) // own_rows)[:, None]
    tp_index = lax.axis_index("tp")
    own_ids = lax.dynamic_slice_in_dim(route_ids, tp_index * own_rows, own_rows, 0)
    own_rank = lax.dynamic_slice_in_dim(slot_rank, tp_index * own_rows, own_rows, 0)
    own_slot = own_ids * slots_each + own_rank
    picker = slot_picker(own_slot, sp_count * slots_each)
    outgoing = jnp.dot(picker, normed, preferred_element_type=jnp.float32).astype(jnp.bfloat16)
    arrived = lax.all_to_all(outgoing, "sp", split_axis=0, concat_axis=0, tiled=True)
    portion = lax.all_gather(arrived, "tp", axis=0, tiled=True)
    gate_pre = jnp.dot(portion, gate_proj[0], preferred_element_type=jnp.float32)
    up_pre = jnp.dot(portion, up_proj[0], preferred_element_type=jnp.float32)
    hidden = clamped_units(gate_pre, up_pre).astype(jnp.bfloat16)
    weight_rows = down_proj[0]
    column_out = jnp.dot(
        lax.all_gather(hidden, "tp", axis=1, tiled=True),
        weight_rows,
        preferred_element_type=jnp.float32,
    ).astype(jnp.bfloat16)
    column_width = column_out.shape[1]
    returned = lax.all_to_all(
        column_out.reshape(tp_count, sp_count, slots_each, column_width),
        "sp",
        split_axis=1,
        concat_axis=1,
        tiled=True,
    )
    home_index = (block_of * sp_count + route_ids) * slots_each + slot_rank
    gathered_out = jnp.take(returned.reshape(-1, column_width), home_index.reshape(-1), axis=0)
    gathered_out = gathered_out.astype(jnp.float32).reshape(seq_rows, top_count, column_width)
    combined_cols = jnp.sum(gathered_out * route_weight[:, :, None], axis=1).astype(jnp.bfloat16)
    combined = lax.all_to_all(combined_cols, "tp", split_axis=0, concat_axis=1, tiled=True)
    layer_out = residual.astype(jnp.float32) + scaled_norm(combined.astype(jnp.float32), post_gain)
    return layer_out.astype(jnp.bfloat16)


def solution(mesh):
    placed = (
        P(("sp", "tp"), None),
        P("sp", "tp"),
        P("sp", "tp"),
        P("sp", "tp"),
        P(None, "tp"),
        P("tp", None),
        P("sp", None),
        P("sp", None),
        P(),
        P(),
        P("sp", None, "tp"),
        P("sp", None, "tp"),
        P("sp", None, "tp"),
    )
    return jax.shard_map(
        local, mesh=mesh, in_specs=placed, out_specs=P(("sp", "tp"), None), check_vma=False
    )
```

profile of v0, /device:TPU:1, one launch (start us, length us, event | category | flops | bytes accessed | tf_op | source)
XLA Modules:
  0.0 329.8 jit_solution(6274343751186609560)
XLA Ops:
  6.6 1.2 multiply_convert_fusion.1
  7.8 3.9 %collective-permute-start = (bf16[2,256]{1,0:T(2,128)(2,1)S(1)}, bf16[2,256]{1,0:T(2,128)(2,1)S(1)}, u32[]{:S(2)}, u32[]{:S(2)}) collective-permute-start(bf16[2,256]{1,0:T(2,128)(2,1)S(1)} %slice.38), channel_id=1, source_target_pairs={{0,4},{4,8},{8,12},{12,16},{16,20},{20,24},{24,28},{1,5},{5,9},{9,... | collective-permute-start | bytes 3080 | tf_op jit(solution)/shard_map/ppermute | solution.py:14
  11.7 0.8 slice_convert_fusion.2
  12.5 3.1 fusion.17
  15.7 0.1 copy.54
  16.1 2.3 reduce-window.6
  18.7 0.1 reshape.118
  19.1 0.1 fusion.9
  19.2 30.4 %reduce-scatter.2.cloned.1.call-done = f32[64,2048]{1,0:T(8,128)} async-done(((f32[256,2048]{1,0:T(8,128)}), f32[64,2048]{1,0:T(8,128)}) %reduce-scatter.2.cloned.1.call-update) | async-done | bytes 524304 | tf_op jit(solution)/shard_map/reduce_scatter | solution.py:80
  49.6 1.2 fusion.5
  50.9 0.8 convolution_convert_fusion.1
  51.7 52.5 %all_to_all.27 = bf16[8,64,2048]{2,1,0:T(8,128)(2,1)} all-to-all(bf16[8,64,2048]{2,1,0:T(8,128)(2,1)S(1)} %bitcast.40), channel_id=1, replica_groups=mesh['sp'=8,'tp'=4] {'sp'}, dimensions={0} | all-to-all | bytes 4194304 | tf_op jit(solution)/shard_map/all_to_all | solution.py:96
  104.2 58.0 %all-gather.3.cloned.1.call-done = bf16[2048,2048]{1,0:T(8,128)(2,1)} async-done(((bf16[512,2048]{1,0:T(8,128)(2,1)}), bf16[2048,2048]{1,0:T(8,128)(2,1)}) %all-gather.3.cloned.1.call-update) | async-done | bytes 8388624 | tf_op jit(solution)/shard_map/all_gather | solution.py:97
  162.3 7.7 %fusion.2 = f32[2048,512]{1,0:T(8,128)S(1)} fusion(bf16[2048,2048]{1,0:T(8,128)(2,1)} %all-gather.3.cloned.1.call-done, bf16[1,2048,512]{2,1,0:T(8,128)(2,1)S(1)} %copy-done), kind=kOutput, calls=%fused_computation.6 | convolution fusion | flops 4294967296 | bytes 14680064 | tf_op jit(solution)/shard_map/dot_general | solution.py:99
  170.0 6.7 %multiply_convert_fusion = bf16[2048,512]{1,0:T(8,128)(2,1)} fusion(f32[2048,512]{1,0:T(8,128)S(1)} %fusion.2, bf16[2048,2048]{1,0:T(8,128)(2,1)S(1)} %copy-done.6, bf16[1,2048,512]{2,1,0:T(8,128)(2,1)S(1)} %copy-done.7), kind=kOutput, calls=%fused_computation.1 | convolution fusion | flops 4305453056 | bytes 16777216 | tf_op jit(solution)/shard_map/dot_general | solution.py:98
  176.7 58.4 %all-gather.5.cloned.1.call-done = bf16[2048,2048]{1,0:T(8,128)(2,1)} async-done(((bf16[2048,512]{1,0:T(8,128)(2,1)}), bf16[2048,2048]{1,0:T(8,128)(2,1)}) %all-gather.5.cloned.1.call-update) | async-done | bytes 8388624 | tf_op jit(solution)/shard_map/all_gather | solution.py:103
  235.1 8.5 %convolution_convert_fusion = bf16[2048,512]{1,0:T(8,128)(2,1)S(1)} fusion(bf16[2048,2048]{1,0:T(8,128)(2,1)} %all-gather.5.cloned.1.call-done, bf16[1,2048,512]{2,1,0:T(8,128)(2,1)} %param.25), kind=kOutput, calls=%fused_computation.2 | convolution fusion | flops 4296015872 | bytes 12582912 | tf_op jit(solution)/shard_map/dot_general | solution.py:102
  243.6 1.4 copy.61
  245.1 5.2 %all-to-all-start.1 = ((bf16[4,8,64,512]{3,2,0,1:T(8,128)(2,1)}), bf16[4,8,64,512]{3,2,0,1:T(8,128)(2,1)}, u32[]{:S(2)}, u32[]{:S(2)}) async-start(bf16[4,8,64,512]{3,2,0,1:T(8,128)(2,1)} %copy.61), calls=%async_computation.2 | async-start | bytes 4194304 | tf_op jit(solution)/shard_map/all_to_all | solution.py:108
  250.3 0.1 copy.63
  250.5 0.1 reshape.121
  250.6 0.8 copy.59
  251.4 0.1 copy.64
  251.5 46.7 %all-to-all-done.1 = bf16[4,8,64,512]{3,2,0,1:T(8,128)(2,1)} async-done(((bf16[4,8,64,512]{3,2,0,1:T(8,128)(2,1)}), bf16[4,8,64,512]{3,2,0,1:T(8,128)(2,1)}, u32[]{:S(2)}, u32[]{:S(2)}) %all-to-all-start.1) | async-done | bytes 2097184 | tf_op jit(solution)/shard_map/all_to_all | solution.py:108
  298.2 3.1 copy.62
  301.4 5.9 %gather_fusion = bf16[1024,512]{1,0:T(8,128)(2,1)S(1)} fusion(bf16[2048,512]{1,0:T(8,128)(2,1)} %bitcast.38, s32[1024]{0:T(1024)S(1)} %broadcast_clamp_fusion), kind=kCustom, calls=%fused_computation | custom fusion | bytes 2101248 | tf_op jit(solution)/shard_map/jit(_take)/gather | solution.py:116
  307.2 1.1 gather.7
  308.3 4.0 %multiply_reduce_fusion = bf16[256,512]{1,0:T(8,128)(2,1)} fusion(f32[256,4]{1,0:T(8,128)S(1)} %copy.64, bf16[256,4,512]{2,1,0:T(4,128)(2,1)} %gather.7, pred[256,4]{1,0:T(8,128)(4,1)} %copy.59), kind=kLoop, calls=%fused_computation.8 | loop fusion | flops 1966080 | bytes 1315840 | tf_op jit(solution)/shard_map/reduce_sum | solution.py:118
  312.3 4.7 %all-to-all-start.2 = ((bf16[4,64,512]{2,1,0:T(8,128)(2,1)}), bf16[4,64,512]{2,1,0:T(8,128)(2,1)S(1)}, u32[]{:S(2)}, u32[]{:S(2)}) async-start(bf16[4,64,512]{2,1,0:T(8,128)(2,1)} %bitcast.14), calls=%async_computation.3 | async-start | bytes 524288 | tf_op jit(solution)/shard_map/all_to_all | solution.py:119
  317.1 5.0 %all-to-all-done.2 = bf16[4,64,512]{2,1,0:T(8,128)(2,1)S(1)} async-done(((bf16[4,64,512]{2,1,0:T(8,128)(2,1)}), bf16[4,64,512]{2,1,0:T(8,128)(2,1)S(1)}, u32[]{:S(2)}, u32[]{:S(2)}) %all-to-all-start.2) | async-done | bytes 262176 | tf_op jit(solution)/shard_map/all_to_all | solution.py:119
  322.2 0.2 fusion.4
  322.4 0.9 fusion.8
  (46 shorter events, 1.1 us)
Async XLA Ops:
  6.5 155.8 %copy-start = (bf16[1,2048,512]{2,1,0:T(8,128)(2,1)S(1)}, bf16[1,2048,512]{2,1,0:T(8,128)(2,1)}, u32[]{:S(2)}) copy-start(bf16[1,2048,512]{2,1,0:T(8,128)(2,1)} %param.24) | copy-start | bytes 6291460
  6.5 9.2 %copy-start.2 = (s32[256,4]{0,1:T(4,128)S(1)}, s32[256,4]{0,1:T(4,128)}, u32[]{:S(2)}) copy-start(s32[256,4]{0,1:T(4,128)} %param.19) | copy-start | bytes 12292
  6.5 12.4 %copy-start.3 = (bf16[2048]{0:T(1024)(128)(2,1)S(1)}, bf16[2048]{0:T(1024)(128)(2,1)}, u32[]{:S(2)}) copy-start(bf16[2048]{0:T(1024)(128)(2,1)} %param.21) | copy-start | bytes 12292
  6.5 43.1 %copy-start.1 = (bf16[64,2048]{1,0:T(8,128)(2,1)S(1)}, bf16[64,2048]{1,0:T(8,128)(2,1)}, u32[]{:S(2)}) copy-start(bf16[64,2048]{1,0:T(8,128)(2,1)} %param.13) | copy-start | bytes 786436
  6.5 43.1 %reduce-scatter.2.cloned.1.call-start = ((), (), s32[]{:S(2)}) async-start(), calls=%async_computation.4 | async-start | bytes 2621440 | tf_op jit(solution)/shard_map/reduce_scatter | solution.py:80
  7.8 4.7 %collective-permute-start = (bf16[2,256]{1,0:T(2,128)(2,1)S(1)}, bf16[2,256]{1,0:T(2,128)(2,1)S(1)}, u32[]{:S(2)}, u32[]{:S(2)}) collective-permute-start(bf16[2,256]{1,0:T(2,128)(2,1)S(1)} %slice.38), channel_id=1, source_target_pairs={{0,4},{4,8},{8,12},{12,16},{16,20},{20,24},{24,28},{1,5},{5,9},{9,... | collective-permute-start | bytes 3080 | tf_op jit(solution)/shard_map/ppermute | solution.py:14
  15.7 146.6 %all-gather.3.cloned.1.call-start = ((), (), s32[]{:S(2)}) async-start(), calls=%async_computation.5 | async-start | bytes 10485760 | tf_op jit(solution)/shard_map/all_gather | solution.py:97
  104.2 130.9 %all-gather.5.cloned.1.call-start = ((), (), s32[]{:S(2)}) async-start(), calls=%async_computation.6 | async-start | bytes 10485760 | tf_op jit(solution)/shard_map/all_gather | solution.py:103
  162.3 7.7 %copy-start.6 = (bf16[2048,2048]{1,0:T(8,128)(2,1)S(1)}, bf16[2048,2048]{1,0:T(8,128)(2,1)}, u32[]{:S(2)}) copy-start(bf16[2048,2048]{1,0:T(8,128)(2,1)} %all-gather.3.cloned.1.call-done) | copy-start | bytes 25165828
  162.3 7.7 %copy-start.7 = (bf16[1,2048,512]{2,1,0:T(8,128)(2,1)S(1)}, bf16[1,2048,512]{2,1,0:T(8,128)(2,1)}, u32[]{:S(2)}) copy-start(bf16[1,2048,512]{2,1,0:T(8,128)(2,1)} %param.23) | copy-start | bytes 6291460
  243.6 7.7 %copy-start.4 = (f32[256,4]{0,1:T(4,128)S(1)}, f32[256,4]{0,1:T(4,128)}, u32[]{:S(2)}) copy-start(f32[256,4]{0,1:T(4,128)} %param.20) | copy-start | bytes 12292
  245.1 53.2 %all-to-all-start.1 = ((bf16[4,8,64,512]{3,2,0,1:T(8,128)(2,1)}), bf16[4,8,64,512]{3,2,0,1:T(8,128)(2,1)}, u32[]{:S(2)}, u32[]{:S(2)}) async-start(bf16[4,8,64,512]{3,2,0,1:T(8,128)(2,1)} %copy.61), calls=%async_computation.2 | async-start | bytes 4194304 | tf_op jit(solution)/shard_map/all_to_all | solution.py:108
  301.4 15.7 %copy-start.5 = (bf16[2048]{0:T(1024)(128)(2,1)S(1)}, bf16[2048]{0:T(1024)(128)(2,1)}, u32[]{:S(2)}) copy-start(bf16[2048]{0:T(1024)(128)(2,1)} %param.22) | copy-start | bytes 12292
  312.3 9.8 %all-to-all-start.2 = ((bf16[4,64,512]{2,1,0:T(8,128)(2,1)}), bf16[4,64,512]{2,1,0:T(8,128)(2,1)S(1)}, u32[]{:S(2)}, u32[]{:S(2)}) async-start(bf16[4,64,512]{2,1,0:T(8,128)(2,1)} %bitcast.14), calls=%async_computation.3 | async-start | bytes 524288 | tf_op jit(solution)/shard_map/all_to_all | solution.py:119
Sparse Core Ops, SparseCore 0:
  15.8 33.7 reduce-scatter.1
  104.3 57.9 all-gather.2
  176.8 58.2 all-gather.4
where the time goes:
time: 331 us; the launch traced here: 330 us
  waiting for transfers between devices  199 us (60%)
  blocking collectives  52.5 us (16%)
  matrix products  26.8 us (8%)
  starting transfers between devices  14 us (4%)
  local copies, waits for them, and re-layouts  13.6 us (4%)
  between operations  13.3 us (4%)
  other arithmetic  10.9 us (3%)
    all_gather x1, waiting for transfers between devices, local(): lax.all_gather(hidden, 'tp', axis=1, tiled=True)  58.4 us
    all_gather x1, waiting for transfers between devices, local(): portion = lax.all_gather(arrived, 'tp', axis=0, tiled=True)  58 us
    all_to_all x1, blocking collectives, local(): lax.all_to_all(outgoing, 'sp', split_axis=0, concat_axis=0, tiled=True)  52.5 us
    all_to_all x1, waiting for transfers between devices, local(): lax.all_to_all(column_out.reshape(tp_count, sp_count, slots_each, column_...  46.7 us
    reduce_scatter x1, waiting for transfers between devices, local(): lax.psum_scatter(jnp.dot(weight_rows, out_weight, preferred_element_type=...  30.4 us
    dot_general x1, matrix products, local(): jnp.dot(lax.all_gather(hidden, 'tp', axis=1, tiled=True), weight_rows, pr...  8.5 us
    dot_general x1, matrix products, local(): up_pre = jnp.dot(portion, up_proj[0], preferred_element_type=jnp.float32)  7.66 us
    gather x2, local copies, waits for them, and re-layouts, local(): jnp.take(returned.reshape(-1, column_width), home_index.reshape(-1), axis=0)  6.98 us
  transfers between devices with their start and end apart: 6, of which 5 were waited for; matrix products, arithmetic and copies ran while one was open for 2% of the time, Pallas kernels for 0%

commit v1 on v0

--- a/solution.py
+++ b/solution.py
@@ -1,6 +1,10 @@
+import functools
+
 import jax
 import jax.numpy as jnp
 from jax import lax
+from jax.experimental import pallas as pl
+from jax.experimental.pallas import tpu as pltpu
 from jax.sharding import PartitionSpec as P
 
 clamp_limit = 7.0
@@ -41,6 +45,489 @@
 def slot_picker(slot_index, table_size):
     matches = slot_index[None, :, :] == jnp.arange(table_size, dtype=jnp.int32)[:, None, None]
     return jnp.any(matches, axis=2).astype(jnp.bfloat16)
+
+
+LANES = 128
+
+
+def table_pick(table, first, second):
+    value = jnp.int32(0)
+    for i, row in enumerate(table):
+        for j, entry in enumerate(row):
+            if entry:
+                value = value + jnp.where((first == i) & (second == j), entry, 0)
+    return value
+
+
+def layer_kernel(
+    sp_count,
+    stream_ref,
+    pre_ref,
+    value_ref,
+    post_ref,
+    taps_ref,
+    ids_ref,
+    weight_ref,
+    gain_ref,
+    post_gain_ref,
+    out_hbm,
+    gate_hbm,
+    up_hbm,
+    down_hbm,
+    result_ref,
+    out_w,
+    gate_w,
+    up_w,
+    down_w,
+    tail,
+    rim,
+    padded,
+    mixed,
+    pair_send,
+    pair_in,
+    own_sum,
+    y_send,
+    y_in,
+    resid,
+    tokens,
+    hidden,
+    part,
+    chain_in,
+    x_in,
+    final,
+    columns,
+    load_sem,
+    rim_sem,
+    proj_sem,
+    y_sem,
+    tok_send,
+    tok_recv,
+    hid_send,
+    hid_recv,
+    chain_send,
+    chain_recv,
+    x_sem,
+    fin_send,
+    fin_recv,
+):
+    f32, bf16 = jnp.float32, jnp.bfloat16
+    heights = sp_count // 2
+    sp = lax.axis_index("sp")
+    tp = lax.axis_index("tp")
+    z, x = lax.div(sp, 2), lax.rem(sp, 2)
+    y, c = lax.div(tp, 2), lax.rem(tp, 2)
+    across, sibling = sp + 1 - 2 * x, tp + 1 - 2 * c
+    opposite = lax.rem(tp + 2, 4)
+    rows, width = stream_ref.shape
+    seq = 4 * rows
+    half = 2 * rows
+    units = gate_w.shape[1]
+
+    def at(sp_to, tp_to):
+        return {"sp": sp_to, "tp": tp_to}
+
+    def remote(source, target, send, receive, device):
+        return pltpu.make_async_remote_copy(
+            src_ref=source,
+            dst_ref=target,
+            send_sem=send,
+            recv_sem=receive,
+            device_id=device,
+            device_id_type=pl.DeviceIdType.MESH,
+        )
+
+    loads = [
+        pltpu.make_async_copy(source, target, load_sem.at[i])
+        for i, (source, target) in enumerate(
+            ((out_hbm, out_w), (gate_hbm.at[0], gate_w), (up_hbm.at[0], up_w), (down_hbm.at[0], down_w))
+        )
+    ]
+    for load in loads:
+        load.start()
+
+    barrier = pltpu.get_barrier_semaphore()
+    partners = [at(lax.rem(sp + by, sp_count), tp) for by in (1, 2, sp_count - 1, sp_count - 2)]
+    partners += [at(across, tp), at(sp, sibling), at(sp, opposite), at(sp, 3 - tp)]
+    for partner in partners:
+        pl.semaphore_signal(barrier, inc=1, device_id=partner, device_id_type=pl.DeviceIdType.MESH)
+    pl.semaphore_wait(barrier, len(partners))
+
+    gated = (pre_ref[...].astype(f32) * value_ref[...].astype(f32)).astype(bf16)
+    tail[...] = gated[seq - 16 :]
+    rim_copy = remote(tail, rim, rim_sem.at[0], rim_sem.at[1], at(lax.rem(sp + 1, sp_count), tp))
+    rim_copy.start()
+    padded[8:, :] = gated.astype(f32)
+    lane = lax.broadcasted_iota(jnp.int32, (rows, LANES), 1)
+    ids = ids_ref[pl.ds(pl.multiple_of(tp * rows, rows), rows), :]
+    weights = weight_ref[pl.ds(pl.multiple_of(tp * rows, rows), rows), :]
+    spread = jnp.zeros((rows, LANES), f32)
+    for k in range(ids.shape[1]):
+        one = weights[:, k : k + 1]
+        high = one.astype(bf16).astype(f32)
+        spread = spread + jnp.where(lane == ids[:, k : k + 1], high, 0.0)
+        spread = spread + jnp.where(lane == ids[:, k : k + 1] + sp_count, one - high, 0.0)
+    own_row = pl.multiple_of(c * half + y * rows, rows)
+    tokens[sp, pl.ds(own_row, rows), width:] = spread.astype(bf16)
+    rim_copy.wait()
+    padded[:8, :] = jnp.where(sp == 0, 0.0, rim[...].astype(f32)[8:])
+    tap_count = taps_ref.shape[0]
+    taps = taps_ref[...].astype(f32)
+    convolved = jnp.zeros((seq, padded.shape[1]), f32)
+    for k in range(tap_count):
+        first = 8 - tap_count + 1 + k
+        convolved = convolved + taps[k : k + 1, :] * padded[first : first + seq, :]
+    mixed[...] = (post_ref[...].astype(f32) * convolved).astype(bf16)
+    loads[0].wait()
+
+    def rows_of(core):
+        return jnp.concatenate(
+            [mixed[pl.ds(pl.multiple_of(yy * half + core * rows, rows), rows), :] for yy in range(2)], 0
+        )
+
+    pair_send[...] = jnp.dot(rows_of(1 - c), out_w[...], preferred_element_type=f32).astype(bf16)
+    pair_copy = remote(pair_send, pair_in, proj_sem.at[0], proj_sem.at[1], at(sp, sibling))
+    pair_copy.start()
+    own_sum[...] = jnp.dot(rows_of(c), out_w[...], preferred_element_type=f32)
+    pair_copy.wait()
+    far = pl.ds(pl.multiple_of((1 - y) * rows, rows), rows)
+    near = pl.ds(pl.multiple_of(y * rows, rows), rows)
+    y_send[...] = (own_sum[far, :] + pair_in[far, :].astype(f32)).astype(bf16)
+    y_copy = remote(y_send, y_in, proj_sem.at[2], proj_sem.at[3], at(sp, opposite))
+    y_copy.start()
+    own_sum[near, :] = own_sum[near, :] + pair_in[near, :].astype(f32)
+    y_copy.wait()
+    residual = (stream_ref[...].astype(f32) + (own_sum[near, :] + y_in[...].astype(f32))).astype(bf16)
+    resid[...] = residual
+    tokens[sp, pl.ds(own_row, rows), :width] = scaled_norm(residual.astype(f32), gain_ref[...]).astype(bf16)
+
+    own_block = tokens.at[sp, pl.ds(own_row, rows), :]
+    block_copy = remote(own_block, own_block, y_sem.at[0], y_sem.at[1], at(sp, opposite))
+    block_copy.start()
+
+    def pair_of(group, core):
+        return tokens.at[group, pl.ds(pl.multiple_of(core * half, half), half), :]
+
+    def forward(way, group):
+        device = (
+            at(lax.rem(sp + 2, sp_count), tp),
+            at(lax.rem(sp + sp_count - 2, sp_count), tp),
+            at(across, tp),
+            at(sp, sibling),
+        )[way]
+        pair = pair_of(group, c)
+        return remote(pair, pair, tok_send.at[way, group], tok_recv.at[group, c], device)
+
+    def arrival(group, core):
+        pair = pair_of(group, core)
+        return remote(pair, pair, tok_send.at[0, group], tok_recv.at[group, core], at(sp, sibling))
+
+    def share(way, group):
+        whose = tp if way < 2 else opposite
+        block = hidden.at[group, whose]
+        return remote(
+            block, block, hid_send.at[way, group], hid_recv.at[group, whose], at(sp, sibling if way else opposite)
+        )
+
+    def shared(group, whose):
+        block = hidden.at[group, whose]
+        return remote(block, block, hid_send.at[0, group], hid_recv.at[group, whose], at(sp, sibling))
+
+    near_first = [sorted(range(heights), key=lambda other: abs(other - i)) for i in range(heights)]
+    far_first = [sorted(range(heights), key=lambda other: -abs(other - i)) for i in range(heights)]
+
+    def group_at(tick):
+        height = table_pick(near_first, z, lax.div(tick, 2))
+        own_x = lax.rem(tick, 2) == 0
+        return height, own_x, 2 * height + jnp.where(own_x, x, 1 - x)
+
+    def homeward(group, down_side):
+        device = at(lax.rem(sp + (sp_count - 2, 2)[down_side], sp_count), tp)
+        return remote(
+            part.at[group],
+            chain_in.at[down_side, group],
+            chain_send.at[group],
+            chain_recv.at[down_side, group],
+            device,
+        )
+
+    def send_home(group, height):
+        @pl.when(height < z)
+        def _():
+            homeward(group, 0).start()
+
+        @pl.when(height > z)
+        def _():
+            homeward(group, 1).start()
+
+    last = heights - 1
+
+    def incoming(height):
+        return ((height < z) & (z < last)) | ((height > z) & (z > 0))
+
+    def take_tokens(tick):
+        height, own_x, group = group_at(tick)
+
+        @pl.when(tick == 0)
+        def _():
+            block_copy.wait_recv()
+
+        @pl.when(tick > 0)
+        def _():
+            arrival(group, c).wait_recv()
+
+        @pl.when(own_x)
+        def _():
+            @pl.when((height <= z) & (z < last))
+            def _():
+                forward(0, group).start()
+
+            @pl.when((height >= z) & (z > 0))
+            def _():
+                forward(1, group).start()
+
+            forward(2, group).start()
+
+        forward(3, group).start()
+        arrival(group, 1 - c).wait_recv()
+
+    def gated_units(tick):
+        _, _, group = group_at(tick)
+        inputs = tokens[group, :, :width]
+        tile = min(256, units)
+        for start in range(0, units, tile):
+            gate_pre = jnp.dot(inputs, gate_w[:, start : start + tile], preferred_element_type=f32)
+            up_pre = jnp.dot(inputs, up_w[:, start : start + tile], preferred_element_type=f32)
+            hidden[group, tp, :, start : start + tile] = clamped_units(gate_pre, up_pre).astype(bf16)
+        share(0, group).start()
+        share(1, group).start()
+
+    def relay_units(tick):
+        _, _, group = group_at(tick)
+        shared(group, opposite).wait_recv()
+        share(2, group).start()
+
+    def project_down(tick):
+        height, _, group = group_at(tick)
+        shared(group, sibling).wait_recv()
+        shared(group, 3 - tp).wait_recv()
+        total = jnp.dot(hidden[group, 0], down_w[:units, :], preferred_element_type=f32)
+        for k in range(1, 4):
+            total = total + jnp.dot(
+                hidden[group, k], down_w[k * units : (k + 1) * units, :], preferred_element_type=f32
+            )
+        lanes = lax.broadcasted_iota(jnp.int32, (seq, LANES), 1)
+        mine = (lanes == sp) | (lanes == sp + sp_count)
+        scale = jnp.sum(jnp.where(mine, tokens[group, :, width:].astype(f32), 0.0), axis=1, keepdims=True)
+        part[group] = (total.astype(bf16).astype(f32) * scale).astype(bf16)
+
+        @pl.when(jnp.logical_not(incoming(height)))
+        def _():
+            send_home(group, height)
+
+    for load in loads[1:]:
+        load.wait()
+
+    def tick_body(tick, carry):
+        @pl.when(tick < sp_count)
+        def _():
+            take_tokens(tick)
+            gated_units(tick)
+
+        @pl.when((tick >= 1) & (tick < sp_count + 1))
+        def _():
+            relay_units(tick - 1)
+
+        @pl.when(tick >= 2)
+        def _():
+            project_down(tick - 2)
+
+        return carry
+
+    lax.fori_loop(0, sp_count + 2, tick_body, 0)
+
+    def came(down_side, group):
+        return remote(
+            part.at[group],
+            chain_in.at[down_side, group],
+            chain_send.at[group],
+            chain_recv.at[down_side, group],
+            at(sp, sibling),
+        )
+
+    def add_in(down_side, group):
+        came(down_side, group).wait_recv()
+        part[group] = (part[group].astype(f32) + chain_in[down_side, group].astype(f32)).astype(bf16)
+
+    def chain_body(item, carry):
+        height = table_pick(far_first, z, lax.div(item, 2))
+        group = 2 * height + lax.rem(item, 2)
+
+        @pl.when(incoming(height))
+        def _():
+            @pl.when(height < z)
+            def _():
+                add_in(0, group)
+
+            @pl.when(height > z)
+            def _():
+                add_in(1, group)
+
+            send_home(group, height)
+
+        return carry
+
+    lax.fori_loop(0, sp_count - 2, chain_body, 0)
+    other = 2 * z + 1 - x
+    x_copy = remote(part.at[other], x_in, x_sem.at[0], x_sem.at[1], at(across, tp))
+    for group in (other, sp):
+        @pl.when(z < last)
+        def _():
+            add_in(0, group)
+
+        @pl.when(z > 0)
+        def _():
+            add_in(1, group)
+
+        if group is other:
+            x_copy.start()
+    x_copy.wait_recv()
+    final[...] = (part[sp].astype(f32) + x_in[...].astype(f32)).astype(bf16)
+
+    def hand_over(step):
+        to = lax.rem(tp + step, 4)
+        begin = pl.multiple_of(lax.rem(to, 2) * half + lax.div(to, 2) * rows, rows)
+        return remote(
+            final.at[pl.ds(begin, rows), :], columns.at[tp], fin_send.at[step - 1], fin_recv.at[tp], at(sp, to)
+        )
+
+    for step in (1, 2, 3):
+        hand_over(step).start()
+    columns[tp] = final[pl.ds(own_row, rows), :]
+    for step in (1, 2, 3):
+        whose = lax.rem(tp + step, 4)
+        remote(
+            final.at[pl.ds(0, rows), :], columns.at[whose], fin_send.at[step - 1], fin_recv.at[whose], at(sp, sibling)
+        ).wait_recv()
+    combined = jnp.concatenate([columns[k] for k in range(4)], 1).astype(f32)
+    result_ref[...] = (resid[...].astype(f32) + scaled_norm(combined, post_gain_ref[...])).astype(bf16)
+
+    block_copy.wait_send()
+    for step in (1, 2, 3):
+        hand_over(step).wait_send()
+    x_copy.wait_send()
+
+    def drain(group, carry):
+        height = lax.div(group, 2)
+
+        @pl.when(lax.rem(group, 2) == x)
+        def _():
+            @pl.when((height <= z) & (z < last))
+            def _():
+                forward(0, group).wait_send()
+
+            @pl.when((height >= z) & (z > 0))
+            def _():
+                forward(1, group).wait_send()
+
+            forward(2, group).wait_send()
+
+        forward(3, group).wait_send()
+        for way in range(3):
+            share(way, group).wait_send()
+
+        @pl.when(height != z)
+        def _():
+            homeward(group, 0).wait_send()
+
+        return carry
+
+    lax.fori_loop(0, sp_count, drain, 0)
+
+
+def dense_layer(
+    stream_in,
+    pre_gate,
+    value_in,
+    post_gate,
+    conv_taps,
+    out_weight,
+    route_ids,
+    route_weight,
+    ffn_gain,
+    post_gain,
+    gate_proj,
+    up_proj,
+    down_proj,
+):
+    sp_count = lax.axis_size("sp")
+    rows, width = stream_in.shape
+    seq, channels = pre_gate.shape
+    units = gate_proj.shape[2]
+    cols = down_proj.shape[2]
+    bf16, f32 = jnp.bfloat16, jnp.float32
+    dma = pltpu.SemaphoreType.DMA
+    scratch = [
+        pltpu.VMEM(out_weight.shape, bf16),
+        pltpu.VMEM(gate_proj.shape[1:], bf16),
+        pltpu.VMEM(up_proj.shape[1:], bf16),
+        pltpu.VMEM(down_proj.shape[1:], bf16),
+        pltpu.VMEM((16, channels), bf16),
+        pltpu.VMEM((16, channels), bf16),
+        pltpu.VMEM((seq + 8, channels), f32),
+        pltpu.VMEM((seq, channels), bf16),
+        pltpu.VMEM((2 * rows, width), bf16),
+        pltpu.VMEM((2 * rows, width), bf16),
+        pltpu.VMEM((2 * rows, width), f32),
+        pltpu.VMEM((rows, width), bf16),
+        pltpu.VMEM((rows, width), bf16),
+        pltpu.VMEM((rows, width), bf16),
+        pltpu.VMEM((sp_count, seq, width + LANES), bf16),
+        pltpu.VMEM((sp_count, 4, seq, units), bf16),
+        pltpu.VMEM((sp_count, seq, cols), bf16),
+        pltpu.VMEM((2, sp_count, seq, cols), bf16),
+        pltpu.VMEM((seq, cols), bf16),
+        pltpu.VMEM((seq, cols), bf16),
+        pltpu.VMEM((4, rows, cols), bf16),
+        dma((4,)),
+        dma((2,)),
+        dma((4,)),
+        dma((2,)),
+        dma((4, sp_count)),
+        dma((sp_count, 2)),
+        dma((3, sp_count)),
+        dma((sp_count, 4)),
+        dma((sp_count,)),
+        dma((2, sp_count)),
+        dma((2,)),
+        dma((3,)),
+        dma((4,)),
+    ]
+    vmem = pl.BlockSpec(memory_space=pltpu.VMEM)
+    anywhere = pl.BlockSpec(memory_space=pl.ANY)
+    return pl.pallas_call(
+        functools.partial(layer_kernel, sp_count),
+        out_shape=jax.ShapeDtypeStruct((rows, width), bf16),
+        in_specs=[vmem] * 9 + [anywhere] * 4,
+        out_specs=vmem,
+        scratch_shapes=scratch,
+        compiler_params=pltpu.CompilerParams(
+            collective_id=0, has_side_effects=True, vmem_limit_bytes=58 * 1024 * 1024
+        ),
+    )(
+        stream_in,
+        pre_gate,
+        value_in,
+        post_gate,
+        conv_taps,
+        route_ids,
+        route_weight,
+        ffn_gain.reshape(1, -1),
+        post_gain.reshape(1, -1),
+        out_weight,
+        gate_proj,
+        up_proj,
+        down_proj,
+    )
 
 
 def local(
@@ -64,6 +551,11 @@
     own_rows = seq_rows // tp_count
     top_count = route_ids.shape[1]
     slots_each = 2 * own_rows * top_count // sp_count
+    if tp_count == 4 and sp_count % 2 == 0 and slots_each >= own_rows:
+        return dense_layer(
+            stream_in, pre_gate, value_in, post_gate, conv_taps, out_weight, route_ids, route_weight,
+            ffn_gain, post_gain, gate_proj, up_proj, down_proj,
+        )
     tap_count = conv_taps.shape[0]
     gated_input = (pre_gate.astype(jnp.float32) * value_in.astype(jnp.float32)).astype(jnp.bfloat16)
     rim_rows = passed_along(gated_input[seq_rows - tap_count + 1 :], "sp", 1)

time: 331 us -> 166 us (0.50)
  the two profiles are of different devices: /device:TPU:1 before, /device:TPU:17 now
where the time goes in v1:
time: 166 us
  Pallas kernels  159 us (96%)
  local copies, waits for them, and re-layouts  7.2 us (4%)
    pallas_call x1, Pallas kernels, dense_layer(): pl.pallas_call(functools.partial(layer_kernel, sp_count), out_shape=jax.S...  159 us
    unnamed x3, local copies, waits for them, and re-layouts  4.63 us

profile of v1, /device:TPU:17, one launch (start us, length us, event | category | flops | bytes accessed | tf_op | source)
XLA Modules:
  0.0 166.0 jit_solution(17758181326952944513)
XLA Ops:
  0.0 1.3 reshape.6.gain_ref
  1.3 1.3 reshape.7.post_gain_ref
  2.6 1.5 copy.14.ids_ref
  4.1 1.5 copy.15.weight_ref
  5.5 158.8 %shard_map.127 = bf16[64,2048]{1,0:T(8,128)(2,1)} custom-call(bf16[64,2048]{1,0:T(8,128)(2,1)} %stream_ref.1, bf16[256,256]{1,0:T(8,128)(2,1)} %pre_ref.1, bf16[256,256]{1,0:T(8,128)(2,1)} %value_ref.1, bf16[256,256]{1,0:T(8,128)(2,1)} %post_ref.1, bf16[3,256]{1,0:T(4,128)(2,1)} %taps_ref.1, s32[256,4]{1,0:T(8,128)} %copy.14.ids_ref, ...), custom_call_target="tpu_custom_call" | custom-call | tf_op jit(solution)/shard_map/pallas_call | solution.py:507
  164.3 1.7 %copy.17 = bf16[64,2048]{1,0:T(8,128)(2,1)} copy(bf16[64,2048]{1,0:T(8,128)(2,1)} %shard_map.127) | data formatting | bytes 524288

commit v2 on v1

--- a/solution.py
+++ b/solution.py
@@ -158,14 +158,22 @@
     rim_copy.start()
     padded[8:, :] = gated.astype(f32)
     lane = lax.broadcasted_iota(jnp.int32, (rows, LANES), 1)
-    ids = ids_ref[pl.ds(pl.multiple_of(tp * rows, rows), rows), :]
-    weights = weight_ref[pl.ds(pl.multiple_of(tp * rows, rows), rows), :]
+    row = lax.broadcasted_iota(jnp.int32, (rows, seq), 0)
+    picked = (lax.broadcasted_iota(jnp.int32, (rows, seq), 1) == row + tp * rows).astype(bf16)
+
+    def own_columns(values):
+        return lax.dot_general(picked, values, (((1,), (1,)), ((), ())), preferred_element_type=f32)
+
+    top_count = ids_ref.shape[0]
+    weights = weight_ref[...]
+    high = weights.astype(bf16)
+    low = own_columns((weights - high.astype(f32)).astype(bf16))
+    high = own_columns(high)
+    ids = own_columns(ids_ref[...].astype(f32).astype(bf16)).astype(jnp.int32)
     spread = jnp.zeros((rows, LANES), f32)
-    for k in range(ids.shape[1]):
-        one = weights[:, k : k + 1]
-        high = one.astype(bf16).astype(f32)
-        spread = spread + jnp.where(lane == ids[:, k : k + 1], high, 0.0)
-        spread = spread + jnp.where(lane == ids[:, k : k + 1] + sp_count, one - high, 0.0)
+    for k in range(top_count):
+        spread = spread + jnp.where(lane == ids[:, k : k + 1], high[:, k : k + 1], 0.0)
+        spread = spread + jnp.where(lane == ids[:, k : k + 1] + sp_count, low[:, k : k + 1], 0.0)
     own_row = pl.multiple_of(c * half + y * rows, rows)
     tokens[sp, pl.ds(own_row, rows), width:] = spread.astype(bf16)
     rim_copy.wait()
@@ -198,28 +206,27 @@
     y_copy.wait()
     residual = (stream_ref[...].astype(f32) + (own_sum[near, :] + y_in[...].astype(f32))).astype(bf16)
     resid[...] = residual
-    tokens[sp, pl.ds(own_row, rows), :width] = scaled_norm(residual.astype(f32), gain_ref[...]).astype(bf16)
-
-    own_block = tokens.at[sp, pl.ds(own_row, rows), :]
-    block_copy = remote(own_block, own_block, y_sem.at[0], y_sem.at[1], at(sp, opposite))
-    block_copy.start()
-
-    def pair_of(group, core):
-        return tokens.at[group, pl.ds(pl.multiple_of(core * half, half), half), :]
-
-    def forward(way, group):
+    tokens[sp, pl.ds(own_row, rows), :width] = scaled_norm(residual.astype(f32), gain_ref[...].reshape(1, width)).astype(bf16)
+
+    def block_of(group, slot):
+        return tokens.at[group, pl.ds(pl.multiple_of(slot * rows, rows), rows), :]
+
+    own_block = block_of(sp, 2 * c + y)
+    block_copy = remote(own_block, own_block, y_sem.at[0], tok_recv.at[sp, 2 * c + y], at(sp, opposite))
+
+    def forward(way, group, yy):
         device = (
             at(lax.rem(sp + 2, sp_count), tp),
             at(lax.rem(sp + sp_count - 2, sp_count), tp),
             at(across, tp),
             at(sp, sibling),
         )[way]
-        pair = pair_of(group, c)
-        return remote(pair, pair, tok_send.at[way, group], tok_recv.at[group, c], device)
-
-    def arrival(group, core):
-        pair = pair_of(group, core)
-        return remote(pair, pair, tok_send.at[0, group], tok_recv.at[group, core], at(sp, sibling))
+        block = block_of(group, 2 * c + yy)
+        return remote(block, block, tok_send.at[way, group, yy], tok_recv.at[group, 2 * c + yy], device)
+
+    def arrival(group, slot):
+        block = block_of(group, slot)
+        return remote(block, block, y_sem.at[0], tok_recv.at[group, slot], at(sp, sibling))
 
     def share(way, group):
         whose = tp if way < 2 else opposite
@@ -233,65 +240,78 @@
         return remote(block, block, hid_send.at[0, group], hid_recv.at[group, whose], at(sp, sibling))
 
     near_first = [sorted(range(heights), key=lambda other: abs(other - i)) for i in range(heights)]
-    far_first = [sorted(range(heights), key=lambda other: -abs(other - i)) for i in range(heights)]
+    home_order = [
+        sorted(
+            range(heights),
+            key=lambda other: (other == i, heights - 1 - i if other < i else i, abs(other - i)),
+        )
+        for i in range(heights)
+    ]
 
     def group_at(tick):
         height = table_pick(near_first, z, lax.div(tick, 2))
         own_x = lax.rem(tick, 2) == 0
-        return height, own_x, 2 * height + jnp.where(own_x, x, 1 - x)
-
-    def homeward(group, down_side):
+        return height, 2 * height + jnp.where(own_x, x, 1 - x)
+
+    def half_of(part_number):
+        return pl.ds(part_number * half, half)
+
+    def homeward(group, down_side, h):
         device = at(lax.rem(sp + (sp_count - 2, 2)[down_side], sp_count), tp)
         return remote(
-            part.at[group],
-            chain_in.at[down_side, group],
-            chain_send.at[group],
-            chain_recv.at[down_side, group],
+            part.at[group, half_of(h), :],
+            chain_in.at[down_side, group, half_of(h), :],
+            chain_send.at[group, h],
+            chain_recv.at[down_side, group, h],
             device,
         )
 
-    def send_home(group, height):
+    def send_home(group, height, h):
         @pl.when(height < z)
         def _():
-            homeward(group, 0).start()
+            homeward(group, 0, h).start()
 
         @pl.when(height > z)
         def _():
-            homeward(group, 1).start()
+            homeward(group, 1, h).start()
 
     last = heights - 1
 
     def incoming(height):
         return ((height < z) & (z < last)) | ((height > z) & (z > 0))
 
-    def take_tokens(tick):
-        height, own_x, group = group_at(tick)
-
-        @pl.when(tick == 0)
-        def _():
-            block_copy.wait_recv()
-
-        @pl.when(tick > 0)
-        def _():
-            arrival(group, c).wait_recv()
-
-        @pl.when(own_x)
-        def _():
-            @pl.when((height <= z) & (z < last))
-            def _():
-                forward(0, group).start()
-
-            @pl.when((height >= z) & (z > 0))
-            def _():
-                forward(1, group).start()
-
-            forward(2, group).start()
-
-        forward(3, group).start()
-        arrival(group, 1 - c).wait_recv()
+    def own_side(step):
+        height = table_pick(near_first, z, lax.div(step, 2))
+        return height, jnp.where(lax.rem(step, 2) == 0, y, 1 - y)
+
+    def take_own(height, yy):
+        group = 2 * height + x
+        arrival(group, 2 * c + yy).wait_recv()
+
+        @pl.when((height <= z) & (z < last))
+        def _():
+            forward(0, group, yy).start()
+
+        @pl.when((height >= z) & (z > 0))
+        def _():
+            forward(1, group, yy).start()
+
+        forward(3, group, yy).start()
+
+    def send_across(step):
+        height, yy = own_side(step)
+        forward(2, 2 * height + x, yy).start()
+
+    def take_across(step):
+        height, yy = own_side(step)
+        group = 2 * height + 1 - x
+        arrival(group, 2 * c + yy).wait_recv()
+        forward(3, group, yy).start()
 
     def gated_units(tick):
-        _, _, group = group_at(tick)
+        _, group = group_at(tick)
+        for yy in range(2):
+            arrival(group, 2 * (1 - c) + yy).wait_recv()
         inputs = tokens[group, :, :width]
         tile = min(256, units)
         for start in range(0, units, tile):
@@ -302,12 +322,12 @@
         share(1, group).start()
 
     def relay_units(tick):
-        _, _, group = group_at(tick)
+        _, group = group_at(tick)
         shared(group, opposite).wait_recv()
         share(2, group).start()
 
     def project_down(tick):
-        height, _, group = group_at(tick)
+        height, group = group_at(tick)
         shared(group, sibling).wait_recv()
         shared(group, 3 - tp).wait_recv()
         total = jnp.dot(hidden[group, 0], down_w[:units, :], preferred_element_type=f32)
@@ -322,122 +342,192 @@
 
         @pl.when(jnp.logical_not(incoming(height)))
         def _():
-            send_home(group, height)
-
+            for h in range(2):
+                send_home(group, height, h)
+
+    block_copy.start()
+    for way, there in ((0, z < last), (1, z > 0)):
+
+        @pl.when(there)
+        def _():
+            forward(way, sp, y).start()
+
+    forward(2, sp, y).start()
+    forward(3, sp, y).start()
+    take_own(z, 1 - y)
+    send_across(jnp.int32(1))
     for load in loads[1:]:
         load.wait()
 
-    def tick_body(tick, carry):
-        @pl.when(tick < sp_count)
-        def _():
-            take_tokens(tick)
-            gated_units(tick)
-
-        @pl.when((tick >= 1) & (tick < sp_count + 1))
-        def _():
-            relay_units(tick - 1)
-
-        @pl.when(tick >= 2)
-        def _():
-            project_down(tick - 2)
+    def take_step(step, yy):
+        distance = lax.div(step, 2) + 1
+
+        @pl.when(z >= distance)
+        def _():
+            take_own(z - distance, yy)
+
+        @pl.when(z + distance <= last)
+        def _():
+            take_own(z + distance, yy)
+
+        send_across(step + 2)
+
+    gated_units(jnp.int32(0))
+
+    def round_body(j, carry):
+        early, late = 2 * j, 2 * j + 1
+
+        @pl.when(j < last)
+        def _():
+            take_step(early, y)
+
+        take_across(early)
+
+        @pl.when(j >= 1)
+        def _():
+            relay_units(early - 1)
+            project_down(early - 2)
+
+        @pl.when(j < last)
+        def _():
+            take_step(late, 1 - y)
+
+        take_across(late)
+        gated_units(late)
+
+        @pl.when(j < last)
+        def _():
+            gated_units(late + 1)
+
+        relay_units(early)
+
+        @pl.when(j >= 1)
+        def _():
+            project_down(early - 1)
 
         return carry
 
-    lax.fori_loop(0, sp_count + 2, tick_body, 0)
-
-    def came(down_side, group):
-        return remote(
-            part.at[group],
-            chain_in.at[down_side, group],
-            chain_send.at[group],
-            chain_recv.at[down_side, group],
+    lax.fori_loop(0, heights, round_body, 0)
+    relay_units(sp_count - 1)
+    project_down(sp_count - 2)
+    project_down(sp_count - 1)
+
+    def add_in(down_side, group, h):
+        remote(
+            part.at[group, half_of(h), :],
+            chain_in.at[down_side, group, half_of(h), :],
+            chain_send.at[group, h],
+            chain_recv.at[down_side, group, h],
             at(sp, sibling),
-        )
-
-    def add_in(down_side, group):
-        came(down_side, group).wait_recv()
-        part[group] = (part[group].astype(f32) + chain_in[down_side, group].astype(f32)).astype(bf16)
+        ).wait_recv()
+        part[group, half_of(h), :] = (
+            part[group, half_of(h), :].astype(f32) + chain_in[down_side, group, half_of(h), :].astype(f32)
+        ).astype(bf16)
 
     def chain_body(item, carry):
-        height = table_pick(far_first, z, lax.div(item, 2))
-        group = 2 * height + lax.rem(item, 2)
+        height = table_pick(home_order, z, lax.div(item, 2))
+        group = 2 * height + jnp.where(lax.rem(item, 2) == 0, x, 1 - x)
 
         @pl.when(incoming(height))
         def _():
-            @pl.when(height < z)
-            def _():
-                add_in(0, group)
-
-            @pl.when(height > z)
-            def _():
-                add_in(1, group)
-
-            send_home(group, height)
+            for h in range(2):
+
+                @pl.when(height < z)
+                def _():
+                    add_in(0, group, h)
+
+                @pl.when(height > z)
+                def _():
+                    add_in(1, group, h)
+
+                send_home(group, height, h)
 
         return carry
 
     lax.fori_loop(0, sp_count - 2, chain_body, 0)
     other = 2 * z + 1 - x
-    x_copy = remote(part.at[other], x_in, x_sem.at[0], x_sem.at[1], at(across, tp))
-    for group in (other, sp):
+
+    def both_sides(group, h):
         @pl.when(z < last)
         def _():
-            add_in(0, group)
+            add_in(0, group, h)
 
         @pl.when(z > 0)
         def _():
-            add_in(1, group)
-
-        if group is other:
-            x_copy.start()
-    x_copy.wait_recv()
-    final[...] = (part[sp].astype(f32) + x_in[...].astype(f32)).astype(bf16)
-
-    def hand_over(step):
-        to = lax.rem(tp + step, 4)
-        begin = pl.multiple_of(lax.rem(to, 2) * half + lax.div(to, 2) * rows, rows)
+            add_in(1, group, h)
+
+    def over_x(h):
         return remote(
-            final.at[pl.ds(begin, rows), :], columns.at[tp], fin_send.at[step - 1], fin_recv.at[tp], at(sp, to)
-        )
-
-    for step in (1, 2, 3):
-        hand_over(step).start()
+            part.at[other, half_of(h), :], x_in.at[half_of(h), :], x_sem.at[0, h], x_sem.at[1, h], at(across, tp)
+        )
+
+    def hand_over(h, yy):
+        return remote(
+            final.at[pl.ds(h * half + yy * rows, rows), :],
+            columns.at[tp],
+            fin_send.at[2 * h + yy],
+            fin_recv.at[tp],
+            at(sp, 2 * yy + h),
+        )
+
+    for h in range(2):
+        both_sides(other, h)
+        over_x(h).start()
+    for h in range(2):
+        both_sides(sp, h)
+        over_x(h).wait_recv()
+        final[half_of(h), :] = (part[sp, half_of(h), :].astype(f32) + x_in[half_of(h), :].astype(f32)).astype(bf16)
+        for yy in range(2):
+
+            @pl.when(tp != 2 * yy + h)
+            def _():
+                hand_over(h, yy).start()
+
     columns[tp] = final[pl.ds(own_row, rows), :]
     for step in (1, 2, 3):
         whose = lax.rem(tp + step, 4)
         remote(
-            final.at[pl.ds(0, rows), :], columns.at[whose], fin_send.at[step - 1], fin_recv.at[whose], at(sp, sibling)
+            final.at[pl.ds(0, rows), :], columns.at[whose], fin_send.at[0], fin_recv.at[whose], at(sp, sibling)
         ).wait_recv()
     combined = jnp.concatenate([columns[k] for k in range(4)], 1).astype(f32)
-    result_ref[...] = (resid[...].astype(f32) + scaled_norm(combined, post_gain_ref[...])).astype(bf16)
+    result_ref[...] = (
+        resid[...].astype(f32) + scaled_norm(combined, post_gain_ref[...].reshape(1, width))
+    ).astype(bf16)
 
     block_copy.wait_send()
-    for step in (1, 2, 3):
-        hand_over(step).wait_send()
-    x_copy.wait_send()
+    for h in range(2):
+        over_x(h).wait_send()
+        for yy in range(2):
+
+            @pl.when(tp != 2 * yy + h)
+            def _():
+                hand_over(h, yy).wait_send()
 
     def drain(group, carry):
         height = lax.div(group, 2)
 
-        @pl.when(lax.rem(group, 2) == x)
-        def _():
-            @pl.when((height <= z) & (z < last))
+        for yy in range(2):
+
+            @pl.when(lax.rem(group, 2) == x)
             def _():
-                forward(0, group).wait_send()
-
-            @pl.when((height >= z) & (z > 0))
-            def _():
-                forward(1, group).wait_send()
-
-            forward(2, group).wait_send()
-
-        forward(3, group).wait_send()
+                @pl.when((height <= z) & (z < last))
+                def _():
+                    forward(0, group, yy).wait_send()
+
+                @pl.when((height >= z) & (z > 0))
+                def _():
+                    forward(1, group, yy).wait_send()
+
+                forward(2, group, yy).wait_send()
+
+            forward(3, group, yy).wait_send()
         for way in range(3):
             share(way, group).wait_send()
 
         @pl.when(height != z)
         def _():
-            homeward(group, 0).wait_send()
+            for h in range(2):
+                homeward(group, 0, h).wait_send()
 
         return carry
 
@@ -491,15 +581,15 @@
         dma((4,)),
         dma((2,)),
         dma((4,)),
-        dma((2,)),
-        dma((4, sp_count)),
-        dma((sp_count, 2)),
+        dma((1,)),
+        dma((4, sp_count, 2)),
+        dma((sp_count, 4)),
         dma((3, sp_count)),
         dma((sp_count, 4)),
-        dma((sp_count,)),
-        dma((2, sp_count)),
-        dma((2,)),
-        dma((3,)),
+        dma((sp_count, 2)),
+        dma((2, sp_count, 2)),
+        dma((2, 2)),
+        dma((4,)),
         dma((4,)),
     ]
     vmem = pl.BlockSpec(memory_space=pltpu.VMEM)
@@ -519,10 +609,10 @@
         value_in,
         post_gate,
         conv_taps,
-        route_ids,
-        route_weight,
-        ffn_gain.reshape(1, -1),
-        post_gain.reshape(1, -1),
+        route_ids.T,
+        route_weight.T,
+        ffn_gain,
+        post_gain,
         out_weight,
         gate_proj,
         up_proj,

time: 166 us -> 123 us (0.74)
  the two profiles are of different devices: /device:TPU:17 before, /device:TPU:1 now
where the time goes in v2:
time: 123 us
  Pallas kernels  121 us (98%)
  local copies, waits for them, and re-layouts  1.67 us (1%)
    pallas_call x1, Pallas kernels, dense_layer(): pl.pallas_call(functools.partial(layer_kernel, sp_count), out_shape=jax.S...  121 us

profile of v2, /device:TPU:1, one launch (start us, length us, event | category | flops | bytes accessed | tf_op | source)
XLA Modules:
  0.0 122.7 jit_solution(14297124505622052807)
XLA Ops:
  0.0 121.1 %shard_map.127 = bf16[64,2048]{1,0:T(8,128)(2,1)} custom-call(bf16[64,2048]{1,0:T(8,128)(2,1)} %stream_ref.1, bf16[256,256]{1,0:T(8,128)(2,1)} %pre_ref.1, bf16[256,256]{1,0:T(8,128)(2,1)} %value_ref.1, bf16[256,256]{1,0:T(8,128)(2,1)} %post_ref.1, bf16[3,256]{1,0:T(4,128)(2,1)} %taps_ref.1, s32[4,256]{1,0:T(4,128)} %bitcast.2, f32[4,256]{1,0:T(4,128)} %bitcast.3, ...), custom_call_target="tpu_custom_call" | custom-call | tf_op jit(solution)/shard_map/pallas_call | solution.py:597
  121.1 1.7 %copy.15 = bf16[64,2048]{1,0:T(8,128)(2,1)} copy(bf16[64,2048]{1,0:T(8,128)(2,1)} %shard_map.127) | data formatting | bytes 524288

commit v3 on v2

--- a/solution.py
+++ b/solution.py
@@ -106,7 +106,8 @@
     hid_recv,
     chain_send,
     chain_recv,
-    x_sem,
+    x_send,
+    x_recv,
     fin_send,
     fin_recv,
 ):
@@ -256,29 +257,26 @@
     def half_of(part_number):
         return pl.ds(part_number * half, half)
 
-    def homeward(group, down_side, h):
+    def over_x(height, h):
+        return remote(
+            part.at[2 * height + 1 - x, half_of(h), :],
+            x_in.at[height, half_of(h), :],
+            x_send.at[height, h],
+            x_recv.at[height, h],
+            at(across, tp),
+        )
+
+    def homeward(height, down_side, h):
         device = at(lax.rem(sp + (sp_count - 2, 2)[down_side], sp_count), tp)
         return remote(
-            part.at[group, half_of(h), :],
-            chain_in.at[down_side, group, half_of(h), :],
-            chain_send.at[group, h],
-            chain_recv.at[down_side, group, h],
+            part.at[2 * height + x, half_of(h), :],
+            chain_in.at[down_side, height, half_of(h), :],
+            chain_send.at[height, h],
+            chain_recv.at[down_side, height, h],
             device,
         )
 
-    def send_home(group, height, h):
-        @pl.when(height < z)
-        def _():
-            homeward(group, 0, h).start()
-
-        @pl.when(height > z)
-        def _():
-            homeward(group, 1, h).start()
-
     last = heights - 1
-
-    def incoming(height):
-        return ((height < z) & (z < last)) | ((height > z) & (z > 0))
 
     def own_side(step):
         height = table_pick(near_first, z, lax.div(step, 2))
@@ -340,10 +338,10 @@
         scale = jnp.sum(jnp.where(mine, tokens[group, :, width:].astype(f32), 0.0), axis=1, keepdims=True)
         part[group] = (total.astype(bf16).astype(f32) * scale).astype(bf16)
 
-        @pl.when(jnp.logical_not(incoming(height)))
+        @pl.when((lax.rem(tick, 2) == 1) & (tick > 1))
         def _():
             for h in range(2):
-                send_home(group, height, h)
+                over_x(height, h).start()
 
     block_copy.start()
     for way, there in ((0, z < last), (1, z > 0)):
@@ -408,58 +406,64 @@
         return carry
 
     lax.fori_loop(0, heights, round_body, 0)
+
+    def f32_half(ref, index, h):
+        return ref[index, half_of(h), :].astype(f32)
+
+    def go_home(item):
+        height = table_pick(home_order, z, item)
+        group = 2 * height + x
+        from_above = (height < z) & (z < last)
+        from_below = (height > z) & (z > 0)
+        for h in range(2):
+            over_x(height, h).wait_recv()
+
+            @pl.when(jnp.logical_not(from_above | from_below))
+            def _():
+                part[group, half_of(h), :] = (f32_half(part, group, h) + f32_half(x_in, height, h)).astype(bf16)
+
+            for down_side, comes in enumerate((from_above, from_below)):
+
+                @pl.when(comes)
+                def _():
+                    homeward(height, down_side, h).wait_recv()
+                    total = f32_half(part, group, h) + f32_half(x_in, height, h)
+                    total = total + chain_in[down_side, height, half_of(h), :].astype(f32)
+                    part[group, half_of(h), :] = total.astype(bf16)
+
+            @pl.when(height < z)
+            def _():
+                homeward(height, 0, h).start()
+
+            @pl.when(height > z)
+            def _():
+                homeward(height, 1, h).start()
+
+    at_end = (z == 0) | (z == last)
+    early_items = min(2, last)
+
+    def go_early(item):
+        @pl.when(at_end)
+        def _():
+            go_home(jnp.int32(item))
+
+    go_early(0)
     relay_units(sp_count - 1)
     project_down(sp_count - 2)
+    if early_items > 1:
+        go_early(1)
     project_down(sp_count - 1)
-
-    def add_in(down_side, group, h):
-        remote(
-            part.at[group, half_of(h), :],
-            chain_in.at[down_side, group, half_of(h), :],
-            chain_send.at[group, h],
-            chain_recv.at[down_side, group, h],
-            at(sp, sibling),
-        ).wait_recv()
-        part[group, half_of(h), :] = (
-            part[group, half_of(h), :].astype(f32) + chain_in[down_side, group, half_of(h), :].astype(f32)
-        ).astype(bf16)
-
-    def chain_body(item, carry):
-        height = table_pick(home_order, z, lax.div(item, 2))
-        group = 2 * height + jnp.where(lax.rem(item, 2) == 0, x, 1 - x)
-
-        @pl.when(incoming(height))
-        def _():
-            for h in range(2):
-
-                @pl.when(height < z)
-                def _():
-                    add_in(0, group, h)
-
-                @pl.when(height > z)
-                def _():
-                    add_in(1, group, h)
-
-                send_home(group, height, h)
+    for h in range(2):
+        over_x(z, h).start()
+
+    def home_body(item, carry):
+        @pl.when(jnp.logical_not(at_end) | (item >= early_items))
+        def _():
+            go_home(item)
 
         return carry
 
-    lax.fori_loop(0, sp_count - 2, chain_body, 0)
-    other = 2 * z + 1 - x
-
-    def both_sides(group, h):
-        @pl.when(z < last)
-        def _():
-            add_in(0, group, h)
-
-        @pl.when(z > 0)
-        def _():
-            add_in(1, group, h)
-
-    def over_x(h):
-        return remote(
-            part.at[other, half_of(h), :], x_in.at[half_of(h), :], x_sem.at[0, h], x_sem.at[1, h], at(across, tp)
-        )
+    lax.fori_loop(0, last, home_body, 0)
 
     def hand_over(h, yy):
         return remote(
@@ -471,12 +475,18 @@
         )
 
     for h in range(2):
-        both_sides(other, h)
-        over_x(h).start()
-    for h in range(2):
-        both_sides(sp, h)
-        over_x(h).wait_recv()
-        final[half_of(h), :] = (part[sp, half_of(h), :].astype(f32) + x_in[half_of(h), :].astype(f32)).astype(bf16)
+        over_x(z, h).wait_recv()
+        part[sp, half_of(h), :] = (f32_half(part, sp, h) + f32_half(x_in, z, h)).astype(bf16)
+        for down_side, comes in enumerate((z < last, z > 0)):
+
+            @pl.when(comes)
+            def _():
+                homeward(z, down_side, h).wait_recv()
+                part[sp, half_of(h), :] = (
+                    f32_half(part, sp, h) + chain_in[down_side, z, half_of(h), :].astype(f32)
+                ).astype(bf16)
+
+        final[half_of(h), :] = part[sp, half_of(h), :]
         for yy in range(2):
 
             @pl.when(tp != 2 * yy + h)
@@ -496,7 +506,6 @@
 
     block_copy.wait_send()
     for h in range(2):
-        over_x(h).wait_send()
         for yy in range(2):
 
             @pl.when(tp != 2 * yy + h)
@@ -524,10 +533,14 @@
         for way in range(3):
             share(way, group).wait_send()
 
-        @pl.when(height != z)
+        @pl.when(lax.rem(group, 2) == 0)
         def _():
             for h in range(2):
-                homeward(group, 0, h).wait_send()
+                over_x(height, h).wait_send()
+
+                @pl.when(height != z)
+                def _():
+                    homeward(height, 0, h).wait_send()
 
         return carry
 
@@ -574,8 +587,8 @@
         pltpu.VMEM((sp_count, seq, width + LANES), bf16),
         pltpu.VMEM((sp_count, 4, seq, units), bf16),
         pltpu.VMEM((sp_count, seq, cols), bf16),
-        pltpu.VMEM((2, sp_count, seq, cols), bf16),
-        pltpu.VMEM((seq, cols), bf16),
+        pltpu.VMEM((2, sp_count // 2, seq, cols), bf16),
+        pltpu.VMEM((sp_count // 2, seq, cols), bf16),
         pltpu.VMEM((seq, cols), bf16),
         pltpu.VMEM((4, rows, cols), bf16),
         dma((4,)),
@@ -586,9 +599,10 @@
         dma((sp_count, 4)),
         dma((3, sp_count)),
         dma((sp_count, 4)),
-        dma((sp_count, 2)),
-        dma((2, sp_count, 2)),
-        dma((2, 2)),
+        dma((sp_count // 2, 2)),
+        dma((2, sp_count // 2, 2)),
+        dma((sp_count // 2, 2)),
+        dma((sp_count // 2, 2)),
         dma((4,)),
         dma((4,)),
     ]

time: 123 us -> 111 us (0.902)
  Pallas kernels: 121 us -> 110 us
    pallas_call x1, Pallas kernels: 121 us -> 110 us  [dense_layer(): pl.pallas_call(functools.partial(layer_kernel, sp_count), out_shape=jax.S...]
where the time goes in v3:
time: 111 us
  Pallas kernels  110 us (99%)
  local copies, waits for them, and re-layouts  1.67 us (2%)
    pallas_call x1, Pallas kernels, dense_layer(): pl.pallas_call(functools.partial(layer_kernel, sp_count), out_shape=jax.S...  110 us

profile of v3, /device:TPU:1, one launch (start us, length us, event | category | flops | bytes accessed | tf_op | source)
XLA Modules:
  0.0 111.2 jit_solution(323551688974188011)
XLA Ops:
  0.0 109.5 %shard_map.127 = bf16[64,2048]{1,0:T(8,128)(2,1)} custom-call(bf16[64,2048]{1,0:T(8,128)(2,1)} %stream_ref.1, bf16[256,256]{1,0:T(8,128)(2,1)} %pre_ref.1, bf16[256,256]{1,0:T(8,128)(2,1)} %value_ref.1, bf16[256,256]{1,0:T(8,128)(2,1)} %post_ref.1, bf16[3,256]{1,0:T(4,128)(2,1)} %taps_ref.1, s32[4,256]{1,0:T(4,128)} %bitcast.2, f32[4,256]{1,0:T(4,128)} %bitcast.3, ...), custom_call_target="tpu_custom_call" | custom-call | tf_op jit(solution)/shard_map/pallas_call | solution.py:611
  109.5 1.7 %copy.15 = bf16[64,2048]{1,0:T(8,128)(2,1)} copy(bf16[64,2048]{1,0:T(8,128)(2,1)} %shard_map.127) | data formatting | bytes 524288
